TPU v7x, 32 devices: a whole 2x2x4 slice. The times are simulated.
32 devices in a mesh: sp: 8 (over z, y), tp: 4 (over x, core).
Axes of the slice: x: 2, y: 2, z: 4, core: 2. Of those that a mesh axis runs over, the one named last changes fastest.
Arguments:
- queries: bfloat16 [4096, 2048], P('sp', 'tp'), may hold values from -8 to 8
- keys: bfloat16 [4096, 512], P('sp', 'tp'), may hold values from -8 to 8
- values: bfloat16 [4096, 512], P('sp', 'tp'), may hold values from -6 to 6
- q_gain: float32 [128], replicated, may hold values from 0.1 to 5.8
- k_gain: float32 [128], replicated, may hold values from 0.1 to 5.8
- out_weight: bfloat16 [2048, 2048], replicated, may hold values from -0.125 to 0.125
- out_gain: float32 [2048], replicated, may hold values from 0.1 to 1.9
- residual_in: bfloat16 [4096, 2048], P(('sp', 'tp')), may hold values from -6 to 6
- mlp_gain: float32 [2048], replicated, may hold values from 0.1 to 1.9
- gate_weight: bfloat16 [2048, 5632], P('sp', 'tp'), may hold values from -0.125 to 0.125
- up_weight: bfloat16 [2048, 5632], P('sp', 'tp'), may hold values from -0.125 to 0.125
- down_weight: bfloat16 [5632, 2048], P('tp', 'sp'), may hold values from -0.078125 to 0.078125
- final_gain: float32 [2048], replicated, may hold values from 0.1 to 1.9
Outputs:
- layer_out: bfloat16 [4096, 2048], P(('sp', 'tp'))
All inputs are finite; a program needn't handle non-finite values.
Results may differ from a plain program's by a relative error of at most 0.015.
The roundings to bfloat16 on the way count: a program that leaves them out, or rounds other values in their place, can miss the bound.
Values may be sent and summed in bfloat16 or wider, within the bound.
A program may use at most 128 MiB of HBM per device.

v0:
```python
import math

import jax
import jax.numpy as jnp
from jax import lax
from jax.sharding import PartitionSpec as P

GRID_W = 64


def rms_scale(matrix):
    return matrix * lax.rsqrt(jnp.mean(matrix * matrix, axis=-1, keepdims=True) + 1e-06)


def rotary(matrix, positions):
    quarter = matrix.shape[-1] // 4
    freqs = 10000.0 ** (-jnp.arange(quarter, dtype=jnp.float32) / quarter)
    grid = jnp.stack([positions // GRID_W, positions % GRID_W], axis=-1).astype(jnp.float32)
    angle = grid[:, :, None] * freqs
    cosine = jnp.cos(angle)[:, None]
    sine = jnp.sin(angle)[:, None]
    parts = matrix.reshape(matrix.shape[:-1] + (2, 2, quarter))
    first = parts[..., 0, :]
    second = parts[..., 1, :]
    turned = jnp.stack([first * cosine - second * sine, second * cosine + first * sine], axis=-2)
    return turned.reshape(matrix.shape)


def on_device(
    queries,
    keys,
    values,
    q_gain,
    k_gain,
    out_weight,
    out_gain,
    residual_in,
    mlp_gain,
    gate_weight,
    up_weight,
    down_weight,
    final_gain,
):
    tok_rows = queries.shape[0]
    head_size = q_gain.shape[0]
    q_heads = queries.shape[1] // head_size
    kv_heads = keys.shape[1] // head_size
    group_size = q_heads // kv_heads
    positions = lax.axis_index("sp") * tok_rows + jnp.arange(tok_rows, dtype=jnp.int32)
    query_rot = rotary(
        rms_scale(queries.reshape(tok_rows, q_heads, head_size).astype(jnp.float32)) * q_gain,
        positions,
    ).astype(jnp.bfloat16)
    key_rot = rotary(
        rms_scale(keys.reshape(tok_rows, kv_heads, head_size).astype(jnp.float32)) * k_gain,
        positions,
    ).astype(jnp.bfloat16)
    key_flat = key_rot.reshape(tok_rows, kv_heads * head_size)
    grouped = query_rot.reshape(tok_rows, kv_heads, group_size, head_size)
    score_scale = head_size ** (-0.5)
    key_all, value_all = (
        lax.all_gather(key_flat, "sp", axis=0, tiled=True),
        lax.all_gather(values, "sp", axis=0, tiled=True),
    )
    total_rows = key_all.shape[0]
    span = math.gcd(total_rows, 1024)
    key_blocks = key_all.reshape(total_rows // span, span, kv_heads, head_size)
    value_blocks = value_all.reshape(total_rows // span, span, kv_heads, head_size)

    def step(run_state, blocks):
        highest, weight_sum, accum = run_state
        key_block, value_block = blocks
        scores = (
            jnp.einsum("qcgd,kcd->cgqk", grouped, key_block, preferred_element_type=jnp.float32)
            * score_scale
        )
        new_high = jnp.maximum(highest, jnp.max(scores, axis=-1))
        factor = jnp.exp(highest - new_high)
        exp_scores = jnp.exp(scores - new_high[..., None])
        weight_sum = weight_sum * factor + jnp.sum(exp_scores, axis=-1)
        accum = accum * factor[..., None] + jnp.einsum(
            "cgqk,kcd->cgqd",
            exp_scores.astype(jnp.bfloat16),
            value_block,
            preferred_element_type=jnp.float32,
        )
        return ((new_high, weight_sum, accum), None)

    start_state = (
        jnp.full((kv_heads, group_size, tok_rows), -1e30, jnp.float32),
        jnp.zeros((kv_heads, group_size, tok_rows), jnp.float32),
        jnp.zeros((kv_heads, group_size, tok_rows, head_size), jnp.float32),
    )
    final_state, unused = lax.scan(step, start_state, (key_blocks, value_blocks))
    highest, weight_sum, accum = final_state
    attended = (
        jnp.transpose(accum / weight_sum[..., None], (2, 0, 1, 3))
        .reshape(tok_rows, q_heads * head_size)
        .astype(jnp.bfloat16)
    )
    head_rows = lax.all_to_all(attended, "tp", split_axis=0, concat_axis=1, tiled=True)
    projected = jnp.dot(head_rows, out_weight, preferred_element_type=jnp.float32)
    mid_stream = (residual_in.astype(jnp.float32) + out_gain * rms_scale(projected)).astype(
        jnp.bfloat16
    )
    normed = (mlp_gain * rms_scale(mid_stream.astype(jnp.float32))).astype(jnp.bfloat16)
    mixer_in = lax.all_gather(normed, "tp", axis=0, tiled=True)
    gate_proj = jnp.dot(
        mixer_in,
        lax.all_gather(gate_weight, "sp", axis=0, tiled=True),
        preferred_element_type=jnp.float32,
    )
    up_proj = jnp.dot(
        mixer_in,
        lax.all_gather(up_weight, "sp", axis=0, tiled=True),
        preferred_element_type=jnp.float32,
    )
    down_full = lax.all_gather(down_weight, "sp", axis=1, tiled=True)
    hidden = (jax.nn.silu(gate_proj) * up_proj).astype(jnp.bfloat16)
    mlp_branch = lax.psum_scatter(
        jnp.dot(hidden, down_full, preferred_element_type=jnp.float32).astype(jnp.bfloat16),
        "tp",
        scatter_dimension=0,
        tiled=True,
    ).astype(jnp.float32)
    return (mid_stream.astype(jnp.float32) + final_gain * rms_scale(mlp_branch)).astype(
        jnp.bfloat16
    )


def solution(mesh):
    return jax.shard_map(
        on_device,
        mesh=mesh,
        in_specs=(
            P("sp", "tp"),
            P("sp", "tp"),
            P("sp", "tp"),
            P(),
            P(),
            P(),
            P(),
            P(("sp", "tp"), None),
            P(),
            P("sp", "tp"),
            P("sp", "tp"),
            P("tp", "sp"),
            P(),
        ),
        out_specs=P(("sp", "tp"), None),
        check_vma=False,
    )
```

profile of v0, /device:TPU:1, one launch (start us, length us, event | category | flops | bytes accessed | tf_op | source)
XLA Modules:
  0.0 512.5 jit_solution(11249257965567632647)
XLA Ops:
  10.5 1.3 copy.18
  13.9 35.0 %all-gather.7.cloned.1.call-done = bf16[4096,128]{0,1:T(8,128)(2,1)} async-done(((bf16[512,128]{0,1:T(8,128)(2,1)}), bf16[4096,128]{0,1:T(8,128)(2,1)}) %all-gather.7.cloned.1.call-update) | async-done | bytes 1048592 | tf_op jit(solution)/shard_map/all_gather | solution.py:62
  48.8 1.6 copy.24
  50.4 40.6 %all-gather.9.cloned.1.call-done = bf16[4096,128]{1,0:T(8,128)(2,1)} async-done(((bf16[512,128]{1,0:T(8,128)(2,1)}), bf16[4096,128]{1,0:T(8,128)(2,1)}) %all-gather.9.cloned.1.call-update) | async-done | bytes 1048592 | tf_op jit(solution)/shard_map/all_gather | solution.py:63
  91.0 47.3 %while.15 = (s32[]{:T(128)}, f32[1,4,512]{2,1,0:T(4,128)S(1)}, f32[1,4,512]{2,1,0:T(4,128)S(1)}, f32[1,4,512,128]{3,2,1,0:T(8,128)S(1)}, bf16[4,1024,1,128]{3,1,...) while((s32[]{:T(128)}, f32[1,4,512]{2,1,0:T(4,128)S(1)}, ...), condition=%wide.region_5.6_spmd.clone, body=%wide.region_2.5_spmd.clone.sunk | while | flops 1091317760 | bytes 61997704 | solution.py:94
  91.0 4.5 bitcast_reduce_fusion.3
  95.5 4.6 fusion.60
  100.1 1.3 copy-done
  101.4 1.4 fusion.59
  102.9 4.5 bitcast_reduce_fusion.3
  107.4 4.6 fusion.60
  112.0 1.3 copy-done
  113.3 1.4 fusion.59
  114.7 4.5 bitcast_reduce_fusion.3
  119.2 4.6 fusion.60
  123.8 1.3 copy-done
  125.1 1.4 fusion.59
  126.5 4.5 bitcast_reduce_fusion.3
  131.0 4.6 fusion.60
  135.6 1.3 copy-done
  136.9 1.4 fusion.59
  139.3 12.7 %all_to_all.16 = bf16[4,128,512]{2,1,0:T(8,128)(2,1)S(1)} all-to-all(bf16[4,128,512]{2,1,0:T(8,128)(2,1)S(1)} %convert_element_type.88), channel_id=1, replica_groups=mesh['sp'=8,'tp'=4] {'tp'}, dimensions={0} | all-to-all | bytes 1048576 | tf_op jit(solution)/shard_map/all_to_all | solution.py:101
  152.3 4.8 multiply_reduce_fusion
  160.5 19.3 %all-gather.11.cloned.1.call-done = bf16[512,2048]{1,0:T(8,128)(2,1)} async-done(((bf16[128,2048]{1,0:T(8,128)(2,1)}), bf16[512,2048]{1,0:T(8,128)(2,1)}) %all-gather.11.cloned.1.call-update) | async-done | bytes 2097168 | tf_op jit(solution)/shard_map/all_gather | solution.py:107
  179.8 92.5 %all-gather.13.cloned.1.call-done = bf16[2048,1408]{1,0:T(8,128)(2,1)} async-done(((bf16[256,1408]{1,0:T(8,128)(2,1)}), bf16[2048,1408]{1,0:T(8,128)(2,1)}) %all-gather.13.cloned.1.call-update) | async-done | bytes 5767184 | tf_op jit(solution)/shard_map/all_gather | solution.py:110
  272.3 8.2 %fusion.43 = f32[512,1408]{1,0:T(8,128)} fusion(bf16[512,2048]{1,0:T(8,128)(2,1)} %all-gather.11.cloned.1.call-done, bf16[2048,1408]{1,0:T(8,128)(2,1)} %all-gather.13.cloned.1.call-done), kind=kOutput, calls=%fused_computation.81 | convolution fusion | flops 2952790016 | bytes 10747904 | tf_op jit(solution)/shard_map/dot_general | solution.py:108
  280.5 84.3 %all-gather.15.cloned.1.call-done = bf16[2048,1408]{1,0:T(8,128)(2,1)} async-done(((bf16[256,1408]{1,0:T(8,128)(2,1)}), bf16[2048,1408]{1,0:T(8,128)(2,1)}) %all-gather.15.cloned.1.call-update) | async-done | bytes 5767184 | tf_op jit(solution)/shard_map/all_gather | solution.py:115
  364.8 94.0 %all-gather.17.cloned.1.call-done = bf16[1408,2048]{1,0:T(8,128)(2,1)} async-done(((bf16[1408,256]{1,0:T(8,128)(2,1)}), bf16[1408,2048]{1,0:T(8,128)(2,1)}) %all-gather.17.cloned.1.call-update) | async-done | bytes 5767184 | tf_op jit(solution)/shard_map/all_gather | solution.py:118
  458.8 13.3 %convolution_convert_fusion = bf16[512,2048]{1,0:T(8,128)(2,1)} fusion(bf16[1408,2048]{1,0:T(8,128)(2,1)} %all-gather.17.cloned.1.call-done, bf16[512,2048]{1,0:T(8,128)(2,1)S(1)} %copy-done.5, bf16[2048,1408]{1,0:T(8,128)(2,1)} %all-gather.15.cloned.1.call-done, f32[512,1408]{1,0:T(8,128)} %fusion.43), kind=kOutput, calls=%fused_computation.28 | convolution fusion | flops 5910953984 | bytes 18612224 | tf_op jit(solution)/shard_map/dot_general | solution.py:121
  472.2 30.1 %reduce-scatter.2.cloned.1.call-done = bf16[128,2048]{1,0:T(8,128)(2,1)} async-done(((bf16[512,2048]{1,0:T(8,128)(2,1)}), bf16[128,2048]{1,0:T(8,128)(2,1)}) %reduce-scatter.2.cloned.1.call-update) | async-done | bytes 524304 | tf_op jit(solution)/shard_map/reduce_scatter | solution.py:120
  502.3 1.2 fusion.25
  503.5 2.1 fusion.30
  (69 shorter events, 10.7 us)
Async XLA Ops:
  6.5 42.3 %all-gather.7.cloned.1.call-start = ((), (), s32[]{:S(2)}) async-start(), calls=%async_computation.2 | async-start | bytes 1179648 | tf_op jit(solution)/shard_map/all_gather | solution.py:62
  9.7 81.4 %all-gather.9.cloned.1.call-start = ((), (), s32[]{:S(2)}) async-start(), calls=%async_computation.3 | async-start | bytes 1179648 | tf_op jit(solution)/shard_map/all_gather | solution.py:63
  10.4 169.4 %all-gather.11.cloned.1.call-start = ((), (), s32[]{:S(2)}) async-start(), calls=%async_computation.4 | async-start | bytes 2621440 | tf_op jit(solution)/shard_map/all_gather | solution.py:107
  95.5 5.9 %copy-start = (f32[1024,512,4]{1,0,2:T(8,128)S(1)}, f32[1024,512,4]{1,0,2:T(8,128)}, u32[]{:S(2)}) copy-start(f32[1024,512,4]{1,0,2:T(8,128)} %get-tuple-element.155) | copy-start | bytes 25165828 | tf_op jit(solution)/shard_map/while
  107.3 5.9 %copy-start = (f32[1024,512,4]{1,0,2:T(8,128)S(1)}, f32[1024,512,4]{1,0,2:T(8,128)}, u32[]{:S(2)}) copy-start(f32[1024,512,4]{1,0,2:T(8,128)} %get-tuple-element.155) | copy-start | bytes 25165828 | tf_op jit(solution)/shard_map/while
  119.2 5.9 %copy-start = (f32[1024,512,4]{1,0,2:T(8,128)S(1)}, f32[1024,512,4]{1,0,2:T(8,128)}, u32[]{:S(2)}) copy-start(f32[1024,512,4]{1,0,2:T(8,128)} %get-tuple-element.155) | copy-start | bytes 25165828 | tf_op jit(solution)/shard_map/while
  131.0 5.9 %copy-start = (f32[1024,512,4]{1,0,2:T(8,128)S(1)}, f32[1024,512,4]{1,0,2:T(8,128)}, u32[]{:S(2)}) copy-start(f32[1024,512,4]{1,0,2:T(8,128)} %get-tuple-element.155) | copy-start | bytes 25165828 | tf_op jit(solution)/shard_map/while
  152.3 4.8 copy-start.1
  152.3 4.8 copy-start.2
  152.3 5.2 %copy-start.3 = (f32[2048]{0:T(1024)S(1)}, f32[2048]{0:T(1024)}, u32[]{:S(2)}) copy-start(f32[2048]{0:T(1024)} %param.23) | copy-start | bytes 24580
  158.5 113.7 %all-gather.13.cloned.1.call-start = ((), (), s32[]{:S(2)}) async-start(), calls=%async_computation.5 | async-start | bytes 6488064 | tf_op jit(solution)/shard_map/all_gather | solution.py:110
  159.1 205.7 %all-gather.15.cloned.1.call-start = ((), (), s32[]{:S(2)}) async-start(), calls=%async_computation.6 | async-start | bytes 6488064 | tf_op jit(solution)/shard_map/all_gather | solution.py:115
  159.7 299.1 %all-gather.17.cloned.1.call-start = ((), (), s32[]{:S(2)}) async-start(), calls=%async_computation.7 | async-start | bytes 6488064 | tf_op jit(solution)/shard_map/all_gather | solution.py:118
  160.3 342.0 %reduce-scatter.2.cloned.1.call-start = ((), (), s32[]{:S(2)}) async-start(), calls=%async_computation.8 | async-start | bytes 2621440 | tf_op jit(solution)/shard_map/reduce_scatter | solution.py:120
  179.8 279.0 %copy-start.5 = (bf16[512,2048]{1,0:T(8,128)(2,1)S(1)}, bf16[512,2048]{1,0:T(8,128)(2,1)}, u32[]{:S(2)}) copy-start(bf16[512,2048]{1,0:T(8,128)(2,1)} %all-gather.11.cloned.1.call-done) | copy-start | bytes 6291460
  280.5 223.0 %copy-start.4 = (f32[2048]{0:T(1024)S(1)}, f32[2048]{0:T(1024)}, u32[]{:S(2)}) copy-start(f32[2048]{0:T(1024)} %param.27) | copy-start | bytes 24580
Sparse Core Ops, SparseCore 0:
  9.8 38.9 all-gather.6
  50.9 40.0 all-gather.8
  158.6 21.1 all-gather.10
  181.8 90.3 all-gather.12
  274.3 90.4 all-gather.14
  366.7 92.0 all-gather.16
  472.3 29.9 reduce-scatter.1
where the time goes:
time: 514 us; the launch traced here: 512 us
  waiting for transfers between devices  398 us (77%)
  matrix products  62.7 us (12%)
  other arithmetic  13.9 us (3%)
  between operations  13.7 us (3%)
  blocking collectives  12.7 us (2%)
  local copies, waits for them, and re-layouts  11 us (2%)
    all_gather x1, waiting for transfers between devices, on_device(): down_full = lax.all_gather(down_weight, 'sp', axis=1, tiled=True)  94 us
    all_gather x1, waiting for transfers between devices, on_device(): lax.all_gather(gate_weight, 'sp', axis=0, tiled=True)  92.5 us
    all_gather x1, waiting for transfers between devices, on_device(): lax.all_gather(up_weight, 'sp', axis=0, tiled=True)  84.3 us
    all_gather x1, waiting for transfers between devices, on_device(): lax.all_gather(values, 'sp', axis=0, tiled=True)  40.6 us
    all_gather x1, waiting for transfers between devices, on_device(): lax.all_gather(key_flat, 'sp', axis=0, tiled=True)  35 us
    reduce_scatter x1, waiting for transfers between devices, on_device(): lax.psum_scatter(jnp.dot(hidden, down_full, preferred_element_type=jnp.fl...  30.1 us
    all_gather x1, waiting for transfers between devices, on_device(): mixer_in = lax.all_gather(normed, 'tp', axis=0, tiled=True)  19.3 us
    dot_general x4, matrix products, step(): jnp.einsum('cgqk,kcd->cgqd', exp_scores.astype(jnp.bfloat16), value_block...  18.4 us
  transfers between devices with their start and end apart: 7, of which 7 were waited for; matrix products, arithmetic and copies ran while one was open for 3% of the time, Pallas kernels for 0%

commit v1 on v0

--- a/solution.py
+++ b/solution.py
@@ -1,8 +1,11 @@
+import functools
 import math
 
 import jax
 import jax.numpy as jnp
 from jax import lax
+from jax.experimental import pallas as pl
+from jax.experimental.pallas import tpu as pltpu
 from jax.sharding import PartitionSpec as P
 
 GRID_W = 64
@@ -128,9 +131,488 @@
     )
 
 
+MESH = pl.DeviceIdType.MESH
+EPS = 1e-06
+
+
+def layer_kernel(
+    n,
+    tn,
+    q_in,
+    k_in,
+    v_hbm,
+    cos_ref,
+    sin_ref,
+    qg_ref,
+    kg_ref,
+    ow_hbm,
+    og_ref,
+    res_ref,
+    mg_ref,
+    gate_hbm,
+    up_hbm,
+    down_hbm,
+    fg_ref,
+    out_ref,
+    qs,
+    kbuf,
+    vbuf,
+    gbuf,
+    ubuf,
+    dbuf,
+    ow,
+    m_s,
+    l_s,
+    acc,
+    att,
+    heads,
+    proj,
+    mid,
+    mix,
+    gacc,
+    uacc,
+    hid,
+    pbuf,
+    rbuf,
+    loc_sem,
+    send_sem,
+    recv_sem,
+    tp_send,
+    tp_recv,
+    pt_send,
+    pt_recv,
+):
+    sp = lax.axis_index("sp")
+    tp = lax.axis_index("tp")
+    half = n // 2
+
+    def ring_at(pos):
+        pos = lax.rem(pos + 2 * n, n)
+        return jnp.where(pos < half, 2 * pos, 2 * (n - 1 - pos) + 1)
+
+    pos = jnp.where(lax.rem(sp, 2) == 0, sp // 2, n - 1 - sp // 2)
+    right, left = ring_at(pos + 1), ring_at(pos - 1)
+    tok, hd = k_in.shape
+    groups = q_in.shape[1] // hd
+    depth = gate_hbm.shape[0]
+    hidden = gate_hbm.shape[1]
+    rows = res_ref.shape[0]
+    width = groups * hd
+
+    locs = {
+        "v": pltpu.make_async_copy(v_hbm, vbuf.at[sp], loc_sem.at[0]),
+        "g": pltpu.make_async_copy(gate_hbm, gbuf.at[sp], loc_sem.at[1]),
+        "u": pltpu.make_async_copy(up_hbm, ubuf.at[sp], loc_sem.at[2]),
+        "d": pltpu.make_async_copy(down_hbm, dbuf.at[sp], loc_sem.at[3]),
+        "o": pltpu.make_async_copy(ow_hbm, ow, loc_sem.at[4]),
+    }
+    for name in "vgudo":
+        locs[name].start()
+
+    lane = lax.broadcasted_iota(jnp.int32, (tok, hd), 1)
+    quarter = hd // 4
+    first = lax.rem(lane, 2 * quarter) < quarter
+
+    def turned(x, gain):
+        x = x.astype(jnp.float32)
+        x = x * lax.rsqrt(jnp.mean(x * x, axis=-1, keepdims=True) + EPS) * gain
+        other = jnp.where(first, pltpu.roll(x, hd - quarter, 1), pltpu.roll(x, quarter, 1))
+        return (x * cos_ref[...] + other * sin_ref[...]).astype(jnp.bfloat16)
+
+    kbuf[sp] = turned(k_in[...], kg_ref[...])
+
+    barrier = pltpu.get_barrier_semaphore()
+    for peer in (left, right):
+        pl.semaphore_signal(barrier, inc=1, device_id=(peer, tp), device_id_type=MESH)
+    for d in range(1, tn):
+        pl.semaphore_signal(
+            barrier, inc=1, device_id=(sp, lax.rem(tp + d, tn)), device_id_type=MESH
+        )
+    pl.semaphore_wait(barrier, 2 + tn - 1)
+
+    cut = hidden // 2
+    items = {
+        "k": (0, half, lambda s: kbuf.at[s]),
+        "v": (1, half - 1, lambda s: vbuf.at[s]),
+        "g": (2, half, lambda s: gbuf.at[s]),
+        "u": (3, half - 1, lambda s: ubuf.at[s]),
+        "a": (4, half, lambda s: dbuf.at[s, pl.ds(0, cut), :]),
+        "b": (5, half - 1, lambda s: dbuf.at[s, pl.ds(cut, hidden - cut), :]),
+    }
+    started = []
+
+    def copies(name, step):
+        number, to_right, view = items[name]
+        found = []
+        for way, count in ((0, to_right), (1, n - 1 - to_right)):
+            if step > count:
+                continue
+            origin = ring_at(pos - (step - 1)) if way == 0 else ring_at(pos + (step - 1))
+            index = (number * 2 + way) * half + step - 1
+            found.append(
+                pltpu.make_async_remote_copy(
+                    src_ref=view(origin),
+                    dst_ref=view(origin),
+                    send_sem=send_sem.at[index],
+                    recv_sem=recv_sem.at[index],
+                    device_id=(right if way == 0 else left, tp),
+                    device_id_type=MESH,
+                )
+            )
+        return found
+
+    def send(name, step):
+        for copy in copies(name, step):
+            copy.start()
+            started.append(copy)
+
+    def arrive(name, step, then=True):
+        number, to_right, view = items[name]
+        for way, count in ((0, to_right), (1, n - 1 - to_right)):
+            if step > count:
+                continue
+            origin = ring_at(pos - step) if way == 0 else ring_at(pos + step)
+            index = (number * 2 + way) * half + step - 1
+            pltpu.make_async_remote_copy(
+                src_ref=view(origin),
+                dst_ref=view(origin),
+                send_sem=send_sem.at[index],
+                recv_sem=recv_sem.at[index],
+                device_id=(right if way == 0 else left, tp),
+                device_id_type=MESH,
+            ).wait_recv()
+            if step < count:
+                index += 1
+                copy = pltpu.make_async_remote_copy(
+                    src_ref=view(origin),
+                    dst_ref=view(origin),
+                    send_sem=send_sem.at[index],
+                    recv_sem=recv_sem.at[index],
+                    device_id=(right if way == 0 else left, tp),
+                    device_id_type=MESH,
+                )
+                copy.start()
+                started.append(copy)
+
+    send("k", 1)
+    locs["v"].wait()
+    send("v", 1)
+    locs["g"].wait()
+    send("g", 1)
+
+    for h in range(groups):
+        qs[h] = turned(q_in[:, h * hd : (h + 1) * hd], qg_ref[...])
+    m_s[...] = jnp.full_like(m_s, -1e30)
+    l_s[...] = jnp.zeros_like(l_s)
+    acc[...] = jnp.zeros_like(acc)
+    factor = hd ** (-0.5) * math.log2(math.e)
+
+    def attend(slots):
+        def one(i, carry):
+            h = lax.rem(i, groups)
+            slot = slots[0]
+            if len(slots) > 1:
+                slot = jnp.where(i < groups, slots[0], slots[1])
+            scores = lax.dot_general(
+                qs[h], kbuf[slot], (((1,), (1,)), ((), ())), preferred_element_type=jnp.float32
+            )
+            before = m_s[h]
+            highest = jnp.maximum(before, jnp.max(scores, axis=-1, keepdims=True))
+            scale = jnp.exp2((before - highest) * factor)
+            probs = jnp.exp2((scores - highest) * factor)
+            m_s[h] = highest
+            l_s[h] = l_s[h] * scale + jnp.sum(probs, axis=-1, keepdims=True)
+            acc[h] = acc[h] * scale + jnp.dot(
+                probs.astype(jnp.bfloat16), vbuf[slot], preferred_element_type=jnp.float32
+            )
+            return carry
+
+        lax.fori_loop(0, groups * len(slots), one, 0)
+
+    attend([sp])
+    for step in range(1, half + 1):
+        arrive("k", step)
+        arrive("v", step)
+        if step == 1:
+            locs["u"].wait()
+            send("u", 1)
+            locs["d"].wait()
+        elif step >= 2:
+            arrive("gu"[step % 2], step // 2 if step % 2 == 0 else (step - 1) // 2)
+        ends = [ring_at(pos - step), ring_at(pos + step)]
+        attend(ends if step < half else ends[:1])
+
+    for h in range(groups):
+        done = (acc[h] / l_s[h]).astype(jnp.bfloat16)
+        for t in range(tn):
+            att[t, :, h * hd : (h + 1) * hd] = done[t * rows : (t + 1) * rows]
+    to_heads = []
+    for d in range(1, tn):
+        peer = lax.rem(tp + d, tn)
+        copy = pltpu.make_async_remote_copy(
+            src_ref=att.at[peer],
+            dst_ref=heads.at[tp],
+            send_sem=tp_send.at[d - 1],
+            recv_sem=tp_recv.at[d - 1],
+            device_id=(sp, peer),
+            device_id_type=MESH,
+        )
+        copy.start()
+        to_heads.append(copy)
+    heads[tp] = att[tp]
+    late = [(name, step) for step in range(1, half + 1) for name in "gu"]
+    seen = [("gu"[s % 2], s // 2 if s % 2 == 0 else (s - 1) // 2) for s in range(2, half + 1)]
+    late = [event for event in late if event not in seen]
+    locs["o"].wait()
+    for copy in to_heads:
+        copy.wait_recv()
+
+    span = math.gcd(ow.shape[1], 512)
+
+    def project(i, carry):
+        cols = pl.ds(pl.multiple_of(i * span, span), span)
+        total = jnp.zeros((rows, span), jnp.float32)
+        for t in range(tn):
+            total += jnp.dot(
+                heads[t], ow[t * width : (t + 1) * width, cols], preferred_element_type=jnp.float32
+            )
+        proj[:, cols] = total
+        return carry
+
+    lax.fori_loop(0, ow.shape[1] // span, project, 0)
+    projected = proj[...]
+    middle = (
+        res_ref[...].astype(jnp.float32)
+        + og_ref[...]
+        * (projected * lax.rsqrt(jnp.mean(projected * projected, axis=-1, keepdims=True) + EPS))
+    ).astype(jnp.bfloat16)
+    mid[...] = middle
+    middle = middle.astype(jnp.float32)
+    normed = (
+        mg_ref[...] * (middle * lax.rsqrt(jnp.mean(middle * middle, axis=-1, keepdims=True) + EPS))
+    ).astype(jnp.bfloat16)
+    mine = pl.ds(pl.multiple_of(tp * rows, rows), rows)
+    for s in range(n):
+        mix[s, mine, :] = normed[:, s * depth : (s + 1) * depth]
+    to_mix = []
+    for d in range(1, tn):
+        peer = lax.rem(tp + d, tn)
+        copy = pltpu.make_async_remote_copy(
+            src_ref=mix.at[:, mine, :],
+            dst_ref=mix.at[:, mine, :],
+            send_sem=tp_send.at[tn - 1 + d - 1],
+            recv_sem=tp_recv.at[tn - 1 + d - 1],
+            device_id=(sp, peer),
+            device_id_type=MESH,
+        )
+        copy.start()
+        to_mix.append(copy)
+
+    for event in late[: len(late) // 2]:
+        arrive(*event)
+    send("a", 1)
+    send("b", 1)
+    gacc[...] = jnp.zeros_like(gacc)
+    uacc[...] = jnp.zeros_like(uacc)
+    for copy in to_mix:
+        copy.wait_recv()
+    tile = math.gcd(tok, 256)
+
+    def add_block(buf, total, slot):
+        def one(i, carry):
+            part = pl.ds(pl.multiple_of(i * tile, tile), tile)
+            total[part, :] += jnp.dot(
+                mix[slot, part, :], buf[slot], preferred_element_type=jnp.float32
+            )
+            return carry
+
+        lax.fori_loop(0, tok // tile, one, 0)
+
+    def add_blocks(name, slots):
+        buf, total = (gbuf, gacc) if name == "g" else (ubuf, uacc)
+        slots = list(slots)
+
+        def one(i, carry):
+            slot = slots[0]
+            for place, other in enumerate(slots[1:]):
+                slot = jnp.where(i > place, other, slot)
+            add_block(buf, total, slot)
+            return carry
+
+        lax.fori_loop(0, len(slots), one, 0)
+
+    def origins(name, step):
+        to_right = items[name][1]
+        found = []
+        if step <= to_right:
+            found.append(ring_at(pos - step))
+        if step <= n - 1 - to_right:
+            found.append(ring_at(pos + step))
+        return found
+
+    ready = {"g": [sp], "u": [sp]}
+    for name, step in seen + late[: len(late) // 2]:
+        ready[name] += origins(name, step)
+    for name in "gu":
+        add_blocks(name, ready[name])
+    for name, step in late[len(late) // 2 :]:
+        arrive(name, step)
+        add_blocks(name, origins(name, step))
+
+    def activate(i, carry):
+        part = pl.ds(pl.multiple_of(i * 64, 64), 64)
+        gate = gacc[part, :]
+        hid[part, :] = (gate / (1.0 + jnp.exp(-gate)) * uacc[part, :]).astype(jnp.bfloat16)
+        return carry
+
+    lax.fori_loop(0, tok // 64, activate, 0)
+
+    def shares(number, slot):
+        def one(t, carry):
+            part = pl.ds(pl.multiple_of(t * rows, rows), rows)
+            pbuf[slot, t] = jnp.dot(
+                hid[part, :], dbuf[slot], preferred_element_type=jnp.float32
+            ).astype(jnp.bfloat16)
+            return carry
+
+        lax.fori_loop(0, tn, one, 0)
+        for d in range(1, tn):
+            peer = lax.rem(tp + d, tn)
+            index = number * (tn - 1) + d - 1
+            copy = pltpu.make_async_remote_copy(
+                src_ref=pbuf.at[slot, peer],
+                dst_ref=rbuf.at[tp, slot],
+                send_sem=pt_send.at[index],
+                recv_sem=pt_recv.at[index],
+                device_id=(sp, peer),
+                device_id_type=MESH,
+            )
+            copy.start()
+            last.append(copy)
+        rbuf[tp, slot] = pbuf[slot, tp]
+
+    last = []
+    shares(0, sp)
+    number = 1
+    for step in range(1, half + 1):
+        arrive("a", step)
+        arrive("b", step)
+        if step < half:
+            for slot in (ring_at(pos - step), ring_at(pos + step)):
+                shares(number, slot)
+                number += 1
+        else:
+            shares(number, ring_at(pos - step))
+    for copy in last:
+        copy.wait_recv()
+    square = jnp.zeros((rows, 1), jnp.float32)
+    for s in range(n):
+        total = rbuf[0, s].astype(jnp.float32)
+        for t in range(1, tn):
+            total += rbuf[t, s].astype(jnp.float32)
+        proj[:, s * depth : (s + 1) * depth] = total
+        square += jnp.sum(total * total, axis=-1, keepdims=True)
+    scale = lax.rsqrt(square / (n * depth) + EPS)
+    out_ref[...] = (mid[...].astype(jnp.float32) + fg_ref[...] * (proj[...] * scale)).astype(
+        jnp.bfloat16
+    )
+    for copy in started + to_heads + to_mix + last:
+        copy.wait_send()
+
+
+def rotary_tables(tok_rows, head_size):
+    quarter = head_size // 4
+    positions = lax.axis_index("sp") * tok_rows + jnp.arange(tok_rows, dtype=jnp.int32)
+    lane = jnp.arange(head_size, dtype=jnp.int32)
+    freqs = 10000.0 ** (-(lane % quarter).astype(jnp.float32) / quarter)
+    row = (positions // GRID_W).astype(jnp.float32)[:, None]
+    column = (positions % GRID_W).astype(jnp.float32)[:, None]
+    angle = jnp.where(lane < 2 * quarter, row, column) * freqs
+    sine = jnp.sin(angle)
+    return jnp.cos(angle), jnp.where(lane % (2 * quarter) < quarter, -sine, sine)
+
+
+def fused(n, tn, *args):
+    (queries, keys, values, q_gain, k_gain, out_weight, out_gain, residual_in) = args[:8]
+    (mlp_gain, gate_weight, up_weight, down_weight, final_gain) = args[8:]
+    tok, hd = keys.shape
+    groups = queries.shape[1] // hd
+    depth, hidden = gate_weight.shape
+    rows, wide = residual_in.shape
+    cosine, sine = rotary_tables(tok, hd)
+    vmem = pl.BlockSpec(memory_space=pltpu.VMEM)
+    hbm = pl.BlockSpec(memory_space=pl.ANY)
+    half = n // 2
+    b16, f32 = jnp.bfloat16, jnp.float32
+    return pl.pallas_call(
+        functools.partial(layer_kernel, n, tn),
+        out_shape=jax.ShapeDtypeStruct((rows, wide), b16),
+        in_specs=[vmem, vmem, hbm, vmem, vmem, vmem, vmem, hbm, vmem, vmem, vmem, hbm, hbm, hbm, vmem],
+        out_specs=vmem,
+        scratch_shapes=[
+            pltpu.VMEM((groups, tok, hd), b16),
+            pltpu.VMEM((n, tok, hd), b16),
+            pltpu.VMEM((n, tok, hd), b16),
+            pltpu.VMEM((n, depth, hidden), b16),
+            pltpu.VMEM((n, depth, hidden), b16),
+            pltpu.VMEM((n, hidden, depth), b16),
+            pltpu.VMEM((wide, wide), b16),
+            pltpu.VMEM((groups, tok, 1), f32),
+            pltpu.VMEM((groups, tok, 1), f32),
+            pltpu.VMEM((groups, tok, hd), f32),
+            pltpu.VMEM((tn, rows, groups * hd), b16),
+            pltpu.VMEM((tn, rows, groups * hd), b16),
+            pltpu.VMEM((rows, wide), f32),
+            pltpu.VMEM((rows, wide), b16),
+            pltpu.VMEM((n, tok, depth), b16),
+            pltpu.VMEM((tok, hidden), f32),
+            pltpu.VMEM((tok, hidden), f32),
+            pltpu.VMEM((tok, hidden), b16),
+            pltpu.VMEM((n, tn, rows, depth), b16),
+            pltpu.VMEM((tn, n, rows, depth), b16),
+            pltpu.SemaphoreType.DMA((5,)),
+            pltpu.SemaphoreType.DMA((12 * half,)),
+            pltpu.SemaphoreType.DMA((12 * half,)),
+            pltpu.SemaphoreType.DMA((2 * (tn - 1),)),
+            pltpu.SemaphoreType.DMA((2 * (tn - 1),)),
+            pltpu.SemaphoreType.DMA((n * (tn - 1),)),
+            pltpu.SemaphoreType.DMA((n * (tn - 1),)),
+        ],
+        compiler_params=pltpu.CompilerParams(
+            collective_id=0, has_side_effects=True, vmem_limit_bytes=67043328
+        ),
+    )(
+        queries,
+        keys,
+        values,
+        cosine,
+        sine,
+        q_gain[None],
+        k_gain[None],
+        out_weight,
+        out_gain[None],
+        residual_in,
+        mlp_gain[None],
+        gate_weight,
+        up_weight,
+        down_weight,
+        final_gain[None],
+    )
+
+
+def body(mesh, *args):
+    n, tn = mesh.shape["sp"], mesh.shape["tp"]
+    tok, hd = args[1].shape
+    depth, hidden = args[9].shape
+    fits = n % 2 == 0 and 4 <= n <= 8 and depth % 128 == 0 and hidden % 32 == 0
+    if fits and tok % 256 == 0 and hd == 128:
+        return fused(n, tn, *args)
+    return on_device(*args)
+
+
 def solution(mesh):
     return jax.shard_map(
-        on_device,
+        functools.partial(body, mesh),
         mesh=mesh,
         in_specs=(
             P("sp", "tp"),

time: 514 us -> 205 us (0.40)
  waiting for transfers between devices: 398 us -> 0 us
  Pallas kernels: 0 us -> 201 us
  matrix products: 62.7 us -> 0 us
  between operations: 13.7 us -> 0.02 us
  blocking collectives: 12.7 us -> 0 us
  other arithmetic: 13.9 us -> 1.88 us
  local copies, waits for them, and re-layouts: 11 us -> 1.88 us
    all_gather x6 -> x0, waiting for transfers between devices: 366 us -> none  [the longest x1 94 us: on_device(): down_full = lax.all_gather(down_weight, 'sp', axis=1, tiled=True)]
    pallas_call x0 -> x1, Pallas kernels: none -> 201 us  [fused(): pl.pallas_call(functools.partial(layer_kernel, n, tn), out_shape=jax.Shap...]
    dot_general x11 -> x0, matrix products: 62.7 us -> none  [the longest x4 18.4 us: step(): jnp.einsum('cgqk,kcd->cgqd', exp_scores.astype(jnp.bfloat16), value_block...]
    reduce_scatter x1 -> x0, waiting for transfers between devices: 30.1 us -> none  [on_device(): lax.psum_scatter(jnp.dot(hidden, down_full, preferred_element_type=jnp.fl...]
    all_to_all x1 -> x0, blocking collectives: 12.7 us -> none  [on_device(): lax.all_to_all(attended, 'tp', split_axis=0, concat_axis=1, tiled=True)]
    reduce_sum x8 -> x0, other arithmetic: 7.32 us -> none  [the longest x4 5.55 us: step(): weight_sum = weight_sum * factor + jnp.sum(exp_scores, axis=-1)]
    while x12 -> x0, local copies, waits for them, and re-layouts: 5.18 us -> none
  transfers between devices with their start and end apart: 7 -> 0, of which waited for: 7 -> 0; matrix products, arithmetic and copies ran while one was open for 3% -> 0% of each run, Pallas kernels for 0% -> 0%
where the time goes in v1:
time: 205 us
  Pallas kernels  201 us (98%)
    pallas_call x1, Pallas kernels, fused(): pl.pallas_call(functools.partial(layer_kernel, n, tn), out_shape=jax.Shap...  201 us

profile of v1, /device:TPU:1, one launch (start us, length us, event | category | flops | bytes accessed | tf_op | source)
XLA Modules:
  0.0 205.0 jit_solution(12052004500420335033)
XLA Ops:
  0.0 1.9 negate_select_fusion
  1.9 201.2 %shard_map.127 = bf16[128,2048]{1,0:T(8,128)(2,1)} custom-call(bf16[512,512]{1,0:T(8,128)(2,1)} %q_in.1, bf16[512,128]{1,0:T(8,128)(2,1)} %k_in.1, bf16[512,128]{1,0:T(8,128)(2,1)} %v_hbm.1, f32[512,128]{1,0:T(8,128)} %get-tuple-element.6.cos_ref, f32[512,128]{1,0:T(8,128)} %get-tuple-element.5.sin_ref, f32[1,128]{1,0:T(1,128)} %bitcast.8, ...), custom_call_target="tpu_custom_call" | custom-call | tf_op jit(solution)/shard_map/pallas_call | solution.py:547
  203.2 1.9 copy.15
  (3 shorter events, 0.0 us)

commit v2 on v1

--- a/solution.py
+++ b/solution.py
@@ -157,9 +157,9 @@
     qs,
     kbuf,
     vbuf,
-    gbuf,
-    ubuf,
-    dbuf,
+    raw,
+    wt,
+    wall,
     ow,
     m_s,
     l_s,
@@ -168,19 +168,23 @@
     heads,
     proj,
     mid,
-    mix,
-    gacc,
-    uacc,
-    hid,
-    pbuf,
-    rbuf,
+    toks,
+    osc,
+    psend,
+    precv,
     loc_sem,
     send_sem,
     recv_sem,
     tp_send,
     tp_recv,
-    pt_send,
-    pt_recv,
+    a_send,
+    a_recv,
+    w_send,
+    w_recv,
+    t_send,
+    t_recv,
+    p_send,
+    p_recv,
 ):
     sp = lax.axis_index("sp")
     tp = lax.axis_index("tp")
@@ -198,12 +202,14 @@
     hidden = gate_hbm.shape[1]
     rows = res_ref.shape[0]
     width = groups * hd
+    chunk = hidden // n
+    side = rows // 2
 
     locs = {
         "v": pltpu.make_async_copy(v_hbm, vbuf.at[sp], loc_sem.at[0]),
-        "g": pltpu.make_async_copy(gate_hbm, gbuf.at[sp], loc_sem.at[1]),
-        "u": pltpu.make_async_copy(up_hbm, ubuf.at[sp], loc_sem.at[2]),
-        "d": pltpu.make_async_copy(down_hbm, dbuf.at[sp], loc_sem.at[3]),
+        "g": pltpu.make_async_copy(gate_hbm, raw.at[0], loc_sem.at[1]),
+        "u": pltpu.make_async_copy(up_hbm, raw.at[1], loc_sem.at[2]),
+        "d": pltpu.make_async_copy(down_hbm, wt.at[2], loc_sem.at[3]),
         "o": pltpu.make_async_copy(ow_hbm, ow, loc_sem.at[4]),
     }
     for name in "vgudo":
@@ -222,22 +228,19 @@
     kbuf[sp] = turned(k_in[...], kg_ref[...])
 
     barrier = pltpu.get_barrier_semaphore()
-    for peer in (left, right):
-        pl.semaphore_signal(barrier, inc=1, device_id=(peer, tp), device_id_type=MESH)
+    for d in range(1, n):
+        pl.semaphore_signal(
+            barrier, inc=1, device_id=(lax.rem(sp + d, n), tp), device_id_type=MESH
+        )
     for d in range(1, tn):
         pl.semaphore_signal(
             barrier, inc=1, device_id=(sp, lax.rem(tp + d, tn)), device_id_type=MESH
         )
-    pl.semaphore_wait(barrier, 2 + tn - 1)
-
-    cut = hidden // 2
+    pl.semaphore_wait(barrier, n - 1 + tn - 1)
+
     items = {
         "k": (0, half, lambda s: kbuf.at[s]),
         "v": (1, half - 1, lambda s: vbuf.at[s]),
-        "g": (2, half, lambda s: gbuf.at[s]),
-        "u": (3, half - 1, lambda s: ubuf.at[s]),
-        "a": (4, half, lambda s: dbuf.at[s, pl.ds(0, cut), :]),
-        "b": (5, half - 1, lambda s: dbuf.at[s, pl.ds(cut, hidden - cut), :]),
     }
     started = []
 
@@ -298,7 +301,75 @@
     locs["v"].wait()
     send("v", 1)
     locs["g"].wait()
-    send("g", 1)
+    locs["u"].wait()
+
+    def transpose(i, carry):
+        part = pl.ds(pl.multiple_of(i * 128, 128), 128)
+        for which in range(2):
+            wt[which, part, :] = raw[which, :, part].T
+        return carry
+
+    lax.fori_loop(0, hidden // 128, transpose, 0)
+    locs["d"].wait()
+
+    def units(index):
+        return pl.ds(pl.multiple_of(index * chunk, 16), chunk)
+
+    own_piece = pltpu.make_async_copy(
+        wt.at[:, units(sp), :], wall.at[sp, :, units(tp), :], loc_sem.at[5]
+    )
+    own_piece.start()
+
+    def spread(d):
+        peer = lax.rem(sp + d, n)
+        copy = pltpu.make_async_remote_copy(
+            src_ref=wt.at[:, units(peer), :],
+            dst_ref=wall.at[sp, :, units(tp), :],
+            send_sem=a_send.at[d - 1],
+            recv_sem=a_recv.at[d - 1],
+            device_id=(peer, tp),
+            device_id_type=MESH,
+        )
+        copy.start()
+        started.append(copy)
+
+    across, beside = lax.rem(tp + tn // 2, tn), tp + 1 - 2 * lax.rem(tp, 2)
+
+    def relay(kind, d):
+        slot = lax.rem(sp - d + n, n)
+        owner = across if kind == 2 else tp
+        piece = wall.at[slot, :, units(owner), :]
+        return pltpu.make_async_remote_copy(
+            src_ref=piece,
+            dst_ref=piece,
+            send_sem=w_send.at[kind * n + d],
+            recv_sem=w_recv.at[kind * n + d],
+            device_id=(sp, across if kind == 0 else beside),
+            device_id_type=MESH,
+        )
+
+    def pass_on(d):
+        if d == 0:
+            own_piece.wait()
+        else:
+            slot = lax.rem(sp - d + n, n)
+            piece = wall.at[slot, :, units(tp), :]
+            pltpu.make_async_remote_copy(
+                src_ref=piece,
+                dst_ref=piece,
+                send_sem=a_send.at[d - 1],
+                recv_sem=a_recv.at[d - 1],
+                device_id=(lax.rem(sp + d, n), tp),
+                device_id_type=MESH,
+            ).wait_recv()
+        for kind in (0, 1):
+            copy = relay(kind, d)
+            copy.start()
+            started.append(copy)
+
+    spread(1)
+    spread(2)
+    pass_on(0)
 
     for h in range(groups):
         qs[h] = turned(q_in[:, h * hd : (h + 1) * hd], qg_ref[...])
@@ -333,14 +404,14 @@
     for step in range(1, half + 1):
         arrive("k", step)
         arrive("v", step)
-        if step == 1:
-            locs["u"].wait()
-            send("u", 1)
-            locs["d"].wait()
-        elif step >= 2:
-            arrive("gu"[step % 2], step // 2 if step % 2 == 0 else (step - 1) // 2)
+        for d in (2 * step + 1, 2 * step + 2):
+            if d < n:
+                spread(d)
         ends = [ring_at(pos - step), ring_at(pos + step)]
         attend(ends if step < half else ends[:1])
+        for d in (2 * step - 5, 2 * step - 4):
+            if 0 < d < n:
+                pass_on(d)
 
     for h in range(groups):
         done = (acc[h] / l_s[h]).astype(jnp.bfloat16)
@@ -360,9 +431,8 @@
         copy.start()
         to_heads.append(copy)
     heads[tp] = att[tp]
-    late = [(name, step) for step in range(1, half + 1) for name in "gu"]
-    seen = [("gu"[s % 2], s // 2 if s % 2 == 0 else (s - 1) // 2) for s in range(2, half + 1)]
-    late = [event for event in late if event not in seen]
+    for d in range(2 * half - 3, n):
+        pass_on(d)
     locs["o"].wait()
     for copy in to_heads:
         copy.wait_recv()
@@ -391,133 +461,113 @@
     normed = (
         mg_ref[...] * (middle * lax.rsqrt(jnp.mean(middle * middle, axis=-1, keepdims=True) + EPS))
     ).astype(jnp.bfloat16)
-    mine = pl.ds(pl.multiple_of(tp * rows, rows), rows)
-    for s in range(n):
-        mix[s, mine, :] = normed[:, s * depth : (s + 1) * depth]
-    to_mix = []
-    for d in range(1, tn):
-        peer = lax.rem(tp + d, tn)
-        copy = pltpu.make_async_remote_copy(
-            src_ref=mix.at[:, mine, :],
-            dst_ref=mix.at[:, mine, :],
-            send_sem=tp_send.at[tn - 1 + d - 1],
-            recv_sem=tp_recv.at[tn - 1 + d - 1],
-            device_id=(sp, peer),
+
+    for way in range(2):
+        toks[way, sp] = normed[way * side : (way + 1) * side]
+
+    def token_copy(way, step):
+        origin = ring_at(pos - (step - 1)) if way == 0 else ring_at(pos + (step - 1))
+        return pltpu.make_async_remote_copy(
+            src_ref=toks.at[way, origin],
+            dst_ref=toks.at[way, origin],
+            send_sem=t_send.at[way * n + step],
+            recv_sem=t_recv.at[way * n + step],
+            device_id=(right if way == 0 else left, tp),
             device_id_type=MESH,
         )
+
+    def sum_copy(way, step):
+        return pltpu.make_async_remote_copy(
+            src_ref=psend.at[way, step],
+            dst_ref=precv.at[way, step],
+            send_sem=p_send.at[way * n + step],
+            recv_sem=p_recv.at[way * n + step],
+            device_id=(right if way == 0 else left, tp),
+            device_id_type=MESH,
+        )
+
+    for way in range(2):
+        token_copy(way, 1).start()
+    for d in range(n):
+        relay(0, d).wait_recv()
+        copy = relay(2, d)
         copy.start()
-        to_mix.append(copy)
-
-    for event in late[: len(late) // 2]:
-        arrive(*event)
-    send("a", 1)
-    send("b", 1)
-    gacc[...] = jnp.zeros_like(gacc)
-    uacc[...] = jnp.zeros_like(uacc)
-    for copy in to_mix:
-        copy.wait_recv()
-    tile = math.gcd(tok, 256)
-
-    def add_block(buf, total, slot):
-        def one(i, carry):
-            part = pl.ds(pl.multiple_of(i * tile, tile), tile)
-            total[part, :] += jnp.dot(
-                mix[slot, part, :], buf[slot], preferred_element_type=jnp.float32
+        started.append(copy)
+    for d in range(n):
+        relay(1, d).wait_recv()
+        relay(2, d).wait_recv()
+
+    def block(step, carry):
+        for way in range(2):
+
+            @pl.when(step > 0)
+            def _():
+                token_copy(way, step).wait_recv()
+
+            @pl.when(jnp.logical_and(step > 0, step < n - 1))
+            def _():
+                token_copy(way, step + 1).start()
+
+        tokens = jnp.concatenate(
+            [toks[0, ring_at(pos - step)], toks[1, ring_at(pos + step)]], axis=0
+        )
+        branches = []
+        for which in range(2):
+            total = jnp.zeros((rows, hidden // n * tn), jnp.float32)
+            for s in range(n):
+                total += lax.dot_general(
+                    tokens[:, s * depth : (s + 1) * depth],
+                    wall[s, which],
+                    (((1,), (1,)), ((), ())),
+                    preferred_element_type=jnp.float32,
+                )
+            branches.append(total)
+        gate, up = branches
+        inner = (gate / (1.0 + jnp.exp(-gate)) * up).astype(jnp.bfloat16)
+        for s in range(n):
+            osc[:, s * depth : (s + 1) * depth] = jnp.dot(
+                inner, wall[s, 2], preferred_element_type=jnp.float32
             )
-            return carry
-
-        lax.fori_loop(0, tok // tile, one, 0)
-
-    def add_blocks(name, slots):
-        buf, total = (gbuf, gacc) if name == "g" else (ubuf, uacc)
-        slots = list(slots)
-
-        def one(i, carry):
-            slot = slots[0]
-            for place, other in enumerate(slots[1:]):
-                slot = jnp.where(i > place, other, slot)
-            add_block(buf, total, slot)
-            return carry
-
-        lax.fori_loop(0, len(slots), one, 0)
-
-    def origins(name, step):
-        to_right = items[name][1]
-        found = []
-        if step <= to_right:
-            found.append(ring_at(pos - step))
-        if step <= n - 1 - to_right:
-            found.append(ring_at(pos + step))
-        return found
-
-    ready = {"g": [sp], "u": [sp]}
-    for name, step in seen + late[: len(late) // 2]:
-        ready[name] += origins(name, step)
-    for name in "gu":
-        add_blocks(name, ready[name])
-    for name, step in late[len(late) // 2 :]:
-        arrive(name, step)
-        add_blocks(name, origins(name, step))
-
-    def activate(i, carry):
-        part = pl.ds(pl.multiple_of(i * 64, 64), 64)
-        gate = gacc[part, :]
-        hid[part, :] = (gate / (1.0 + jnp.exp(-gate)) * uacc[part, :]).astype(jnp.bfloat16)
+
+        @pl.when(step == 0)
+        def _():
+            proj[...] = osc[...]
+
+        @pl.when(step > 0)
+        def _():
+            for way in range(2):
+                part = slice(way * side, (way + 1) * side)
+
+                @pl.when(step > 1)
+                def _():
+                    sum_copy(way, step - 1).wait_recv()
+                    osc[part] += precv[way, step - 1].astype(jnp.float32)
+
+                psend[way, step] = osc[part].astype(jnp.bfloat16)
+                sum_copy(way, step).start()
+
         return carry
 
-    lax.fori_loop(0, tok // 64, activate, 0)
-
-    def shares(number, slot):
-        def one(t, carry):
-            part = pl.ds(pl.multiple_of(t * rows, rows), rows)
-            pbuf[slot, t] = jnp.dot(
-                hid[part, :], dbuf[slot], preferred_element_type=jnp.float32
-            ).astype(jnp.bfloat16)
-            return carry
-
-        lax.fori_loop(0, tn, one, 0)
-        for d in range(1, tn):
-            peer = lax.rem(tp + d, tn)
-            index = number * (tn - 1) + d - 1
-            copy = pltpu.make_async_remote_copy(
-                src_ref=pbuf.at[slot, peer],
-                dst_ref=rbuf.at[tp, slot],
-                send_sem=pt_send.at[index],
-                recv_sem=pt_recv.at[index],
-                device_id=(sp, peer),
-                device_id_type=MESH,
-            )
-            copy.start()
-            last.append(copy)
-        rbuf[tp, slot] = pbuf[slot, tp]
-
-    last = []
-    shares(0, sp)
-    number = 1
-    for step in range(1, half + 1):
-        arrive("a", step)
-        arrive("b", step)
-        if step < half:
-            for slot in (ring_at(pos - step), ring_at(pos + step)):
-                shares(number, slot)
-                number += 1
-        else:
-            shares(number, ring_at(pos - step))
-    for copy in last:
-        copy.wait_recv()
-    square = jnp.zeros((rows, 1), jnp.float32)
-    for s in range(n):
-        total = rbuf[0, s].astype(jnp.float32)
-        for t in range(1, tn):
-            total += rbuf[t, s].astype(jnp.float32)
-        proj[:, s * depth : (s + 1) * depth] = total
-        square += jnp.sum(total * total, axis=-1, keepdims=True)
-    scale = lax.rsqrt(square / (n * depth) + EPS)
-    out_ref[...] = (mid[...].astype(jnp.float32) + fg_ref[...] * (proj[...] * scale)).astype(
-        jnp.bfloat16
-    )
-    for copy in started + to_heads + to_mix + last:
+    lax.fori_loop(0, n, block, 0)
+    for way in range(2):
+        sum_copy(way, n - 1).wait_recv()
+        part = slice(way * side, (way + 1) * side)
+        proj[part] += precv[way, n - 1].astype(jnp.float32)
+    total = proj[...]
+    out_ref[...] = (
+        mid[...].astype(jnp.float32)
+        + fg_ref[...] * (total * lax.rsqrt(jnp.mean(total * total, axis=-1, keepdims=True) + EPS))
+    ).astype(jnp.bfloat16)
+    for copy in started + to_heads:
         copy.wait_send()
+
+    def drain(step, carry):
+        for way in range(2):
+            token_copy(way, step).wait_send()
+            sum_copy(way, step).wait_send()
+        return carry
+
+    lax.fori_loop(1, n, drain, 0)
 
 
 def rotary_tables(tok_rows, head_size):
@@ -553,9 +603,9 @@
             pltpu.VMEM((groups, tok, hd), b16),
             pltpu.VMEM((n, tok, hd), b16),
             pltpu.VMEM((n, tok, hd), b16),
-            pltpu.VMEM((n, depth, hidden), b16),
-            pltpu.VMEM((n, depth, hidden), b16),
-            pltpu.VMEM((n, hidden, depth), b16),
+            pltpu.VMEM((2, depth, hidden), b16),
+            pltpu.VMEM((3, hidden, depth), b16),
+            pltpu.VMEM((n, 3, hidden // n * tn, depth), b16),
             pltpu.VMEM((wide, wide), b16),
             pltpu.VMEM((groups, tok, 1), f32),
             pltpu.VMEM((groups, tok, 1), f32),
@@ -564,19 +614,23 @@
             pltpu.VMEM((tn, rows, groups * hd), b16),
             pltpu.VMEM((rows, wide), f32),
             pltpu.VMEM((rows, wide), b16),
-            pltpu.VMEM((n, tok, depth), b16),
-            pltpu.VMEM((tok, hidden), f32),
-            pltpu.VMEM((tok, hidden), f32),
-            pltpu.VMEM((tok, hidden), b16),
-            pltpu.VMEM((n, tn, rows, depth), b16),
-            pltpu.VMEM((tn, n, rows, depth), b16),
-            pltpu.SemaphoreType.DMA((5,)),
-            pltpu.SemaphoreType.DMA((12 * half,)),
-            pltpu.SemaphoreType.DMA((12 * half,)),
-            pltpu.SemaphoreType.DMA((2 * (tn - 1),)),
-            pltpu.SemaphoreType.DMA((2 * (tn - 1),)),
-            pltpu.SemaphoreType.DMA((n * (tn - 1),)),
-            pltpu.SemaphoreType.DMA((n * (tn - 1),)),
+            pltpu.VMEM((2, n, rows // 2, wide), b16),
+            pltpu.VMEM((rows, wide), f32),
+            pltpu.VMEM((2, n, rows // 2, wide), b16),
+            pltpu.VMEM((2, n, rows // 2, wide), b16),
+            pltpu.SemaphoreType.DMA((6,)),
+            pltpu.SemaphoreType.DMA((4 * half,)),
+            pltpu.SemaphoreType.DMA((4 * half,)),
+            pltpu.SemaphoreType.DMA((tn - 1,)),
+            pltpu.SemaphoreType.DMA((tn - 1,)),
+            pltpu.SemaphoreType.DMA((n - 1,)),
+            pltpu.SemaphoreType.DMA((n - 1,)),
+            pltpu.SemaphoreType.DMA((3 * n,)),
+            pltpu.SemaphoreType.DMA((3 * n,)),
+            pltpu.SemaphoreType.DMA((2 * n,)),
+            pltpu.SemaphoreType.DMA((2 * n,)),
+            pltpu.SemaphoreType.DMA((2 * n,)),
+            pltpu.SemaphoreType.DMA((2 * n,)),
         ],
         compiler_params=pltpu.CompilerParams(
             collective_id=0, has_side_effects=True, vmem_limit_bytes=67043328
@@ -604,7 +658,8 @@
     n, tn = mesh.shape["sp"], mesh.shape["tp"]
     tok, hd = args[1].shape
     depth, hidden = args[9].shape
-    fits = n % 2 == 0 and 4 <= n <= 8 and depth % 128 == 0 and hidden % 32 == 0
+    fits = n % 2 == 0 and 4 <= n <= 8 and depth % 128 == 0 and hidden % 128 == 0
+    fits = fits and tn == 4 and hidden % (16 * n) == 0 and args[7].shape[0] % 32 == 0
     if fits and tok % 256 == 0 and hd == 128:
         return fused(n, tn, *args)
     return on_device(*args)

time: 205 us -> 215 us (1.049); the launches traced: 205 us -> 212 us
  Pallas kernels: 201 us -> 208 us
    pallas_call x1, Pallas kernels: 201 us -> 208 us  [fused(): pl.pallas_call(functools.partial(layer_kernel, n, tn), out_shape=jax.Shap...]
where the time goes in v2:
time: 215 us; the launch traced here: 212 us
  Pallas kernels  208 us (97%)
    pallas_call x1, Pallas kernels, fused(): pl.pallas_call(functools.partial(layer_kernel, n, tn), out_shape=jax.Shap...  208 us

profile of v2, /device:TPU:1, one launch (start us, length us, event | category | flops | bytes accessed | tf_op | source)
XLA Modules:
  0.0 211.8 jit_solution(15836255444106876130)
XLA Ops:
  0.0 1.9 negate_select_fusion
  1.9 208.0 %shard_map.127 = bf16[128,2048]{1,0:T(8,128)(2,1)} custom-call(bf16[512,512]{1,0:T(8,128)(2,1)} %q_in.1, bf16[512,128]{1,0:T(8,128)(2,1)} %k_in.1, bf16[512,128]{1,0:T(8,128)(2,1)} %v_hbm.1, f32[512,128]{1,0:T(8,128)} %get-tuple-element.6.cos_ref, f32[512,128]{1,0:T(8,128)} %get-tuple-element.5.sin_ref, f32[1,128]{1,0:T(1,128)} %bitcast.8, ...), custom_call_target="tpu_custom_call" | custom-call | tf_op jit(solution)/shard_map/pallas_call | solution.py:597
  209.9 1.9 copy.15
  (3 shorter events, 0.0 us)

commit v3 on v1

--- a/solution.py
+++ b/solution.py
@@ -141,8 +141,6 @@
     q_in,
     k_in,
     v_hbm,
-    cos_ref,
-    sin_ref,
     qg_ref,
     kg_ref,
     ow_hbm,
@@ -154,6 +152,8 @@
     down_hbm,
     fg_ref,
     out_ref,
+    cos_ref,
+    sin_ref,
     qs,
     kbuf,
     vbuf,
@@ -219,8 +219,6 @@
         other = jnp.where(first, pltpu.roll(x, hd - quarter, 1), pltpu.roll(x, quarter, 1))
         return (x * cos_ref[...] + other * sin_ref[...]).astype(jnp.bfloat16)
 
-    kbuf[sp] = turned(k_in[...], kg_ref[...])
-
     barrier = pltpu.get_barrier_semaphore()
     for peer in (left, right):
         pl.semaphore_signal(barrier, inc=1, device_id=(peer, tp), device_id_type=MESH)
@@ -294,11 +292,21 @@
                 copy.start()
                 started.append(copy)
 
-    send("k", 1)
+    for name in "gu":
+        locs[name].wait()
+        send(name, 1)
+
+    place = sp * tok + lax.broadcasted_iota(jnp.int32, (tok, hd), 0)
+    place = jnp.where(lane < 2 * quarter, place // GRID_W, lax.rem(place, GRID_W))
+    turn = lax.rem(lane, quarter).astype(jnp.float32)
+    angle = place.astype(jnp.float32) * jnp.exp(turn * (-math.log(10000.0) / quarter))
+    cos_ref[...] = jnp.cos(angle)
+    sine = jnp.sin(angle)
+    sin_ref[...] = jnp.where(first, -sine, sine)
+    kbuf[sp] = turned(k_in[...], kg_ref[...])
     locs["v"].wait()
     send("v", 1)
-    locs["g"].wait()
-    send("g", 1)
+    send("k", 1)
 
     for h in range(groups):
         qs[h] = turned(q_in[:, h * hd : (h + 1) * hd], qg_ref[...])
@@ -331,14 +339,11 @@
 
     attend([sp])
     for step in range(1, half + 1):
+        arrive("ug"[step % 2], (step + 1) // 2)
         arrive("k", step)
         arrive("v", step)
         if step == 1:
-            locs["u"].wait()
-            send("u", 1)
             locs["d"].wait()
-        elif step >= 2:
-            arrive("gu"[step % 2], step // 2 if step % 2 == 0 else (step - 1) // 2)
         ends = [ring_at(pos - step), ring_at(pos + step)]
         attend(ends if step < half else ends[:1])
 
@@ -361,7 +366,7 @@
         to_heads.append(copy)
     heads[tp] = att[tp]
     late = [(name, step) for step in range(1, half + 1) for name in "gu"]
-    seen = [("gu"[s % 2], s // 2 if s % 2 == 0 else (s - 1) // 2) for s in range(2, half + 1)]
+    seen = [("ug"[s % 2], (s + 1) // 2) for s in range(1, half + 1)]
     late = [event for event in late if event not in seen]
     locs["o"].wait()
     for copy in to_heads:
@@ -520,18 +525,6 @@
         copy.wait_send()
 
 
-def rotary_tables(tok_rows, head_size):
-    quarter = head_size // 4
-    positions = lax.axis_index("sp") * tok_rows + jnp.arange(tok_rows, dtype=jnp.int32)
-    lane = jnp.arange(head_size, dtype=jnp.int32)
-    freqs = 10000.0 ** (-(lane % quarter).astype(jnp.float32) / quarter)
-    row = (positions // GRID_W).astype(jnp.float32)[:, None]
-    column = (positions % GRID_W).astype(jnp.float32)[:, None]
-    angle = jnp.where(lane < 2 * quarter, row, column) * freqs
-    sine = jnp.sin(angle)
-    return jnp.cos(angle), jnp.where(lane % (2 * quarter) < quarter, -sine, sine)
-
-
 def fused(n, tn, *args):
     (queries, keys, values, q_gain, k_gain, out_weight, out_gain, residual_in) = args[:8]
     (mlp_gain, gate_weight, up_weight, down_weight, final_gain) = args[8:]
@@ -539,7 +532,6 @@
     groups = queries.shape[1] // hd
     depth, hidden = gate_weight.shape
     rows, wide = residual_in.shape
-    cosine, sine = rotary_tables(tok, hd)
     vmem = pl.BlockSpec(memory_space=pltpu.VMEM)
     hbm = pl.BlockSpec(memory_space=pl.ANY)
     half = n // 2
@@ -547,9 +539,11 @@
     return pl.pallas_call(
         functools.partial(layer_kernel, n, tn),
         out_shape=jax.ShapeDtypeStruct((rows, wide), b16),
-        in_specs=[vmem, vmem, hbm, vmem, vmem, vmem, vmem, hbm, vmem, vmem, vmem, hbm, hbm, hbm, vmem],
+        in_specs=[vmem, vmem, hbm, vmem, vmem, hbm, vmem, vmem, vmem, hbm, hbm, hbm, vmem],
         out_specs=vmem,
         scratch_shapes=[
+            pltpu.VMEM((tok, hd), f32),
+            pltpu.VMEM((tok, hd), f32),
             pltpu.VMEM((groups, tok, hd), b16),
             pltpu.VMEM((n, tok, hd), b16),
             pltpu.VMEM((n, tok, hd), b16),
@@ -585,8 +579,6 @@
         queries,
         keys,
         values,
-        cosine,
-        sine,
         q_gain[None],
         k_gain[None],
         out_weight,

time: 205 us -> 201 us (0.980)
    pallas_call x1, Pallas kernels: 201 us -> 199 us  [fused(): pl.pallas_call(functools.partial(layer_kernel, n, tn), out_shape=jax.Shap...]
where the time goes in v3:
time: 201 us
  Pallas kernels  199 us (99%)
    pallas_call x1, Pallas kernels, fused(): pl.pallas_call(functools.partial(layer_kernel, n, tn), out_shape=jax.Shap...  199 us

profile of v3, /device:TPU:1, one launch (start us, length us, event | category | flops | bytes accessed | tf_op | source)
XLA Modules:
  0.0 201.0 jit_solution(12642257626417398251)
XLA Ops:
  0.0 199.1 %shard_map.127 = bf16[128,2048]{1,0:T(8,128)(2,1)} custom-call(bf16[512,512]{1,0:T(8,128)(2,1)} %q_in.1, bf16[512,128]{1,0:T(8,128)(2,1)} %k_in.1, bf16[512,128]{1,0:T(8,128)(2,1)} %v_hbm.1, f32[1,128]{1,0:T(1,128)} %bitcast.8, f32[1,128]{1,0:T(1,128)} %bitcast.9, bf16[2048,2048]{1,0:T(8,128)(2,1)} %ow_hbm.1, f32[1,2048]{1,0:T(1,128)} %bitcast.5, ...), custom_call_target="tpu_custom_call" | custom-call | tf_op jit(solution)/shard_map/pallas_call | solution.py:539
  199.1 1.9 copy.15
